TPU v7x, 32 devices: a whole 2x2x4 slice. The times are simulated.
32 devices in a mesh: row: 4 (over y, x), col: 8 (over z, core).
Axes of the slice: x: 2, y: 2, z: 4, core: 2. Of those that a mesh axis runs over, the one named last changes fastest.
Arguments:
- tokens: bfloat16 [2, 2048, 1024], P(None, ('row', 'col')), may hold values from -6 to 6
- proj_weight: bfloat16 [1024, 256], replicated, may hold values from -0.1875 to 0.1875
- gate_weight: bfloat16 [1024, 256], replicated, may hold values from -0.1875 to 0.1875
- out_weight: bfloat16 [256, 1024], replicated, may hold values from -0.375 to 0.375
Outputs:
- mixed_out: bfloat16 [2, 2048, 1024], P(None, ('col', 'row'))
All inputs are finite; a program needn't handle non-finite values.
Results may differ from a plain program's by a relative error of at most 0.02.
Values may be sent and summed in bfloat16 or wider, within the bound.
A program may use at most 64 MiB of HBM per device.

v0:
```python
import math

import jax
import jax.numpy as jnp
from jax import lax
from jax.sharding import PartitionSpec as P

GROUPS = 4
GROUP_DIM = 64


def as_sent(x):
    return jax.tree.map(lambda a: a.astype(jnp.bfloat16) if a.dtype == jnp.float32 else a, x)


def channel_tables(table_size):
    index_vec = jnp.arange(table_size, dtype=jnp.int32)
    turns_mod = index_vec[:, None] * index_vec[None, :] % table_size
    angles = 2.0 * math.pi / table_size * turns_mod.astype(jnp.float32)
    norm_scale = 1.0 / math.sqrt(table_size)
    return (jnp.cos(angles) * norm_scale, jnp.sin(angles) * norm_scale)


def channel_section(mix_input):
    seq_count, tok_rows = (mix_input.shape[0], mix_input.shape[1])
    grouped = mix_input.astype(jnp.float32).reshape(seq_count, tok_rows, GROUPS, GROUP_DIM)
    cos_table, sin_table = channel_tables(GROUP_DIM)
    real_part = jnp.einsum("stgn,nk->tsgk", grouped, cos_table, precision=lax.Precision.HIGHEST)
    imag_part = -jnp.einsum("stgn,nk->tsgk", grouped, sin_table, precision=lax.Precision.HIGHEST)
    return (real_part.reshape(tok_rows, -1), imag_part.reshape(tok_rows, -1))


def row_factor(real_part, imag_part, col_start, length_all):
    row_count, tok_rows, col_width = real_part.shape
    cos_table, sin_table = channel_tables(row_count)
    cos_table = cos_table * math.sqrt(row_count)
    sin_table = sin_table * math.sqrt(row_count)
    high = lax.Precision.HIGHEST
    first_real = jnp.einsum("ka,atm->ktm", cos_table, real_part, precision=high) + jnp.einsum(
        "ka,atm->ktm", sin_table, imag_part, precision=high
    )
    first_imag = jnp.einsum("ka,atm->ktm", cos_table, imag_part, precision=high) - jnp.einsum(
        "ka,atm->ktm", sin_table, real_part, precision=high
    )
    index_vec = jnp.arange(row_count, dtype=jnp.int32)
    position = col_start + jnp.arange(tok_rows, dtype=jnp.int32)
    turns_mod = index_vec[:, None] * position[None, :] % length_all
    angles = 2.0 * math.pi / length_all * turns_mod.astype(jnp.float32)
    twiddle_cos = jnp.cos(angles)[:, :, None]
    twiddle_sin = jnp.sin(angles)[:, :, None]
    turned_real = twiddle_cos * first_real + twiddle_sin * first_imag
    turned_imag = twiddle_cos * first_imag - twiddle_sin * first_real
    merged_real = jnp.transpose(turned_real, (1, 0, 2)).reshape(tok_rows, row_count * col_width)
    merged_imag = jnp.transpose(turned_imag, (1, 0, 2)).reshape(tok_rows, row_count * col_width)
    return (merged_real, merged_imag)


def dense_section(real_part, imag_part, length_all):
    length = real_part.shape[0]
    block_rows = min(512, length)
    block_count = length // block_rows
    points = jnp.arange(length, dtype=jnp.int32)

    def one_block(block_start):
        freq_index = block_start + jnp.arange(block_rows, dtype=jnp.int32)
        turns_mod = freq_index[:, None] * points[None, :] % length
        angles = 2.0 * math.pi / length * turns_mod.astype(jnp.float32)
        first = jnp.dot(
            jnp.cos(angles),
            real_part,
            precision=lax.Precision.HIGHEST,
            preferred_element_type=jnp.float32,
        )
        second = jnp.dot(
            jnp.sin(angles),
            imag_part,
            precision=lax.Precision.HIGHEST,
            preferred_element_type=jnp.float32,
        )
        return first + second

    starts = jnp.arange(block_count, dtype=jnp.int32) * block_rows
    spectrum = lax.map(one_block, starts).reshape(length, real_part.shape[1])
    return (spectrum * (1.0 / math.sqrt(length_all))).astype(jnp.bfloat16)


def local_order(returned, row_count):
    tok_rows = returned.shape[0]
    return returned.reshape(tok_rows, row_count, -1).reshape(tok_rows * row_count, -1)


def body(tokens, proj_weight, gate_weight, out_weight):
    seq_count, tok_rows, model_width = tokens.shape
    flattened = tokens.reshape(seq_count * tok_rows, model_width)
    hidden = jnp.dot(flattened, proj_weight, preferred_element_type=jnp.float32).astype(
        jnp.bfloat16
    )
    gate_pre = jnp.dot(flattened, gate_weight, preferred_element_type=jnp.float32)
    mix_input = (hidden.astype(jnp.float32) * jax.nn.silu(gate_pre)).astype(jnp.bfloat16)
    real_part, imag_part = channel_section(mix_input.reshape(seq_count, tok_rows, -1))
    row_count = lax.axis_size("row")
    length_all = row_count * lax.axis_size("col") * tok_rows
    col_start = lax.axis_index("col") * tok_rows
    received = (
        lax.all_to_all(as_sent(real_part[None]), "row", split_axis=2, concat_axis=0, tiled=True),
        lax.all_to_all(as_sent(imag_part[None]), "row", split_axis=2, concat_axis=0, tiled=True),
    )
    merged_real, merged_imag = row_factor(received[0], received[1], col_start, length_all)
    moved_pair = (
        lax.all_to_all(as_sent(merged_real), "col", split_axis=1, concat_axis=0, tiled=True).astype(
            merged_real.dtype
        ),
        lax.all_to_all(as_sent(merged_imag), "col", split_axis=1, concat_axis=0, tiled=True).astype(
            merged_imag.dtype
        ),
    )
    spectrum = dense_section(moved_pair[0], moved_pair[1], length_all)
    returned = lax.all_to_all(spectrum, "col", split_axis=0, concat_axis=1, tiled=True)
    mixed_cols = lax.all_to_all(
        local_order(returned, row_count), "row", split_axis=0, concat_axis=1, tiled=True
    )
    mixed = mixed_cols.reshape(tok_rows, seq_count, -1)
    result_out = jnp.einsum("tsc,cd->std", mixed, out_weight, preferred_element_type=jnp.float32)
    return result_out.astype(jnp.bfloat16)


def solution(mesh):
    in_specs = (P(None, ("row", "col"), None), P(), P(), P())
    out_specs = P(None, ("col", "row"), None)
    return jax.shard_map(body, mesh=mesh, in_specs=in_specs, out_specs=out_specs, check_vma=False)
```

profile of v0, /device:TPU:0, one launch (start us, length us, event | category | flops | bytes accessed | tf_op | source)
XLA Modules:
  0.0 73.3 jit_solution(7594770349935760409)
XLA Ops:
  0.0 1.5 %fusion.98 = f32[128,256]{1,0:T(8,128)S(1)} fusion(bf16[128,1024]{1,0:T(8,128)(2,1)} %bitcast.95, bf16[1024,256]{1,0:T(8,128)(2,1)} %param.6), kind=kOutput, calls=%fused_computation.116 | convolution fusion | flops 67108864 | bytes 917504 | tf_op jit(solution)/shard_map/dot_general | solution.py:98
  1.9 0.6 convolution_convert_fusion.1
  2.6 0.5 broadcast.201
  3.1 1.4 %reduce.1 = bf16[512,64]{1,0:T(8,128)(2,1)S(1)} reduce(bf16[512,1,64]{2,1,0:T(2,128)(2,1)S(1)} %bitcast.89, bf16[]{:T(256)} %broadcast.201), dimensions={1}, to_apply=%bitcast.86.reduce_sub_computation | reduce | bytes 131074
  4.6 0.8 %reshape.130 = bf16[4,2,4096]{2,1,0:T(2,128)(2,1)} reshape(bf16[512,64]{1,0:T(8,128)(2,1)S(1)} %reduce.1) | data formatting | bytes 131072
  5.4 5.2 %all-to-all-start = ((bf16[4,2,4096]{2,1,0:T(2,128)(2,1)}), bf16[4,2,4096]{2,1,0:T(2,128)(2,1)S(1)}, u32[]{:S(2)}, u32[]{:S(2)}) async-start(bf16[4,2,4096]{2,1,0:T(2,128)(2,1)} %reshape.130), calls=%async_computation | async-start | bytes 131072 | tf_op jit(solution)/shard_map/all_to_all | solution.py:105
  10.6 0.6 fusion.1
  11.6 1.4 %reduce = bf16[512,64]{1,0:T(8,128)(2,1)S(1)} reduce(bf16[512,1,64]{2,1,0:T(2,128)(2,1)S(1)} %bitcast.90, bf16[]{:T(256)} %broadcast.201), dimensions={1}, to_apply=%bitcast.85.reduce_sub_computation | reduce | bytes 131074
  13.1 0.8 %reshape.128 = bf16[4,2,4096]{2,1,0:T(2,128)(2,1)} reshape(bf16[512,64]{1,0:T(8,128)(2,1)S(1)} %reduce) | data formatting | bytes 131072
  13.9 1.6 %all-to-all-done = bf16[4,2,4096]{2,1,0:T(2,128)(2,1)S(1)} async-done(((bf16[4,2,4096]{2,1,0:T(2,128)(2,1)}), bf16[4,2,4096]{2,1,0:T(2,128)(2,1)S(1)}, u32[]{:S(2)}, u32[]{:S(2)}) %all-to-all-start) | async-done | bytes 65568 | tf_op jit(solution)/shard_map/all_to_all | solution.py:105
  15.5 3.3 %all-to-all-start.1 = ((bf16[4,2,4096]{2,1,0:T(2,128)(2,1)}), bf16[4,2,4096]{2,1,0:T(2,128)(2,1)S(1)}, u32[]{:S(2)}, u32[]{:S(2)}) async-start(bf16[4,2,4096]{2,1,0:T(2,128)(2,1)} %reshape.128), calls=%async_computation.1 | async-start | bytes 131072 | tf_op jit(solution)/shard_map/all_to_all | solution.py:106
  19.4 4.2 %all-to-all-done.1 = bf16[4,2,4096]{2,1,0:T(2,128)(2,1)S(1)} async-done(((bf16[4,2,4096]{2,1,0:T(2,128)(2,1)}), bf16[4,2,4096]{2,1,0:T(2,128)(2,1)S(1)}, u32[]{:S(2)}, u32[]{:S(2)}) %all-to-all-start.1) | async-done | bytes 65568 | tf_op jit(solution)/shard_map/all_to_all | solution.py:106
  24.5 0.4 subtract_convert_fusion
  25.0 0.8 %reshape.134 = bf16[8,2,2048]{2,1,0:T(2,128)(2,1)} reshape(bf16[8,64,64]{2,1,0:T(8,128)(2,1)S(1)} %bitcast.91) | data formatting | bytes 131072
  25.8 4.9 %all-to-all-start.3 = ((bf16[8,2,2048]{2,1,0:T(2,128)(2,1)}), bf16[8,2,2048]{2,1,0:T(2,128)(2,1)S(1)}, u32[]{:S(2)}, u32[]{:S(2)}) async-start(bf16[8,2,2048]{2,1,0:T(2,128)(2,1)} %reshape.134), calls=%async_computation.3 | async-start | bytes 131072 | tf_op jit(solution)/shard_map/all_to_all | solution.py:113
  30.8 0.8 %reshape.132 = bf16[8,2,2048]{2,1,0:T(2,128)(2,1)} reshape(bf16[8,64,64]{2,1,0:T(8,128)(2,1)S(1)} %bitcast.92) | data formatting | bytes 131072
  31.6 5.0 %all-to-all-done.3 = bf16[8,2,2048]{2,1,0:T(2,128)(2,1)S(1)} async-done(((bf16[8,2,2048]{2,1,0:T(2,128)(2,1)}), bf16[8,2,2048]{2,1,0:T(2,128)(2,1)S(1)}, u32[]{:S(2)}, u32[]{:S(2)}) %all-to-all-start.3) | async-done | bytes 65568 | tf_op jit(solution)/shard_map/all_to_all | solution.py:113
  36.6 3.4 %all-to-all-start.2 = ((bf16[8,2,2048]{2,1,0:T(2,128)(2,1)}), bf16[8,2,2048]{2,1,0:T(2,128)(2,1)S(1)}, u32[]{:S(2)}, u32[]{:S(2)}) async-start(bf16[8,2,2048]{2,1,0:T(2,128)(2,1)} %reshape.132), calls=%async_computation.2 | async-start | bytes 131072 | tf_op jit(solution)/shard_map/all_to_all | solution.py:110
  40.4 5.4 %all-to-all-done.2 = bf16[8,2,2048]{2,1,0:T(2,128)(2,1)S(1)} async-done(((bf16[8,2,2048]{2,1,0:T(2,128)(2,1)}), bf16[8,2,2048]{2,1,0:T(2,128)(2,1)S(1)}, u32[]{:S(2)}, u32[]{:S(2)}) %all-to-all-start.2) | async-done | bytes 65568 | tf_op jit(solution)/shard_map/all_to_all | solution.py:110
  46.2 4.7 %fusion.13 = f32[512,64]{0,1:T(8,128)S(1)} fusion(bf16[512,64]{0,1:T(8,128)(2,1)S(1)} %all_to_all.82), kind=kOutput, calls=%fused_computation.23 | convolution fusion | flops 204996608 | bytes 196608 | tf_op jit(solution)/shard_map/while/body/eval_jaxpr/dot_general | solution.py:68
  50.9 5.1 %fusion.5 = bf16[512,64]{0,1:T(8,128)(2,1)S(1)} fusion(f32[512,64]{0,1:T(8,128)S(1)} %fusion.13, bf16[512,64]{0,1:T(8,128)(2,1)S(1)} %all_to_all.85), kind=kOutput, calls=%fused_computation.14 | convolution fusion | flops 205094912 | bytes 262144 | tf_op jit(solution)/shard_map/while/body/eval_jaxpr/dot_general | solution.py:74
  56.3 8.3 %all_to_all.97 = bf16[8,2,2048]{2,1,0:T(2,128)(2,1)S(1)} all-to-all(bf16[8,2,2048]{2,1,0:T(2,128)(2,1)S(1)} %reshape.136), channel_id=1, replica_groups=mesh['row'=4,'col'=8] {'col'}, dimensions={0} | all-to-all | bytes 131072 | tf_op jit(solution)/shard_map/all_to_all | solution.py:118
  65.0 7.2 %all_to_all.98 = bf16[4,64,128]{2,1,0:T(8,128)(2,1)S(1)} all-to-all(bf16[4,64,128]{2,1,0:T(8,128)(2,1)S(1)} %all_to_all.88), channel_id=1, replica_groups=mesh['row'=4,'col'=8] {'row'}, dimensions={0} | all-to-all | bytes 131072 | tf_op jit(solution)/shard_map/all_to_all | solution.py:119
  72.3 0.9 %fusion = bf16[2,64,1024]{2,1,0:T(8,128)(2,1)} fusion(bf16[256,1024]{1,0:T(8,128)(2,1)S(1)} %copy-done, bf16[64,2,256]{2,1,0:T(2,128)(2,1)S(1)} %reshape.122), kind=kOutput, calls=%fused_computation.4 | convolution fusion | flops 67239936 | bytes 851968 | tf_op jit(solution)/shard_map/tsc,cd->std/dot_general | solution.py:123
  (40 shorter events, 4.3 us)
Async XLA Ops:
  0.0 72.3 %copy-start = (bf16[256,1024]{1,0:T(8,128)(2,1)S(1)}, bf16[256,1024]{1,0:T(8,128)(2,1)}, u32[]{:S(2)}) copy-start(bf16[256,1024]{1,0:T(8,128)(2,1)} %param.7) | copy-start | bytes 1572868
  0.0 1.5 %copy-start.2 = (bf16[1024,256]{1,0:T(8,128)(2,1)S(1)}, bf16[1024,256]{1,0:T(8,128)(2,1)}, u32[]{:S(2)}) copy-start(bf16[1024,256]{1,0:T(8,128)(2,1)} %param.5) | copy-start | bytes 1572868
  0.0 1.5 %copy-start.1 = (bf16[2,64,1024]{2,1,0:T(8,128)(2,1)S(1)}, bf16[2,64,1024]{2,1,0:T(8,128)(2,1)}, u32[]{:S(2)}) copy-start(bf16[2,64,1024]{2,1,0:T(8,128)(2,1)} %param.4) | copy-start | bytes 786436
  5.4 10.1 %all-to-all-start = ((bf16[4,2,4096]{2,1,0:T(2,128)(2,1)}), bf16[4,2,4096]{2,1,0:T(2,128)(2,1)S(1)}, u32[]{:S(2)}, u32[]{:S(2)}) async-start(bf16[4,2,4096]{2,1,0:T(2,128)(2,1)} %reshape.130), calls=%async_computation | async-start | bytes 131072 | tf_op jit(solution)/shard_map/all_to_all | solution.py:105
  15.5 8.1 %all-to-all-start.1 = ((bf16[4,2,4096]{2,1,0:T(2,128)(2,1)}), bf16[4,2,4096]{2,1,0:T(2,128)(2,1)S(1)}, u32[]{:S(2)}, u32[]{:S(2)}) async-start(bf16[4,2,4096]{2,1,0:T(2,128)(2,1)} %reshape.128), calls=%async_computation.1 | async-start | bytes 131072 | tf_op jit(solution)/shard_map/all_to_all | solution.py:106
  25.8 10.8 %all-to-all-start.3 = ((bf16[8,2,2048]{2,1,0:T(2,128)(2,1)}), bf16[8,2,2048]{2,1,0:T(2,128)(2,1)S(1)}, u32[]{:S(2)}, u32[]{:S(2)}) async-start(bf16[8,2,2048]{2,1,0:T(2,128)(2,1)} %reshape.134), calls=%async_computation.3 | async-start | bytes 131072 | tf_op jit(solution)/shard_map/all_to_all | solution.py:113
  36.6 9.2 %all-to-all-start.2 = ((bf16[8,2,2048]{2,1,0:T(2,128)(2,1)}), bf16[8,2,2048]{2,1,0:T(2,128)(2,1)S(1)}, u32[]{:S(2)}, u32[]{:S(2)}) async-start(bf16[8,2,2048]{2,1,0:T(2,128)(2,1)} %reshape.132), calls=%async_computation.2 | async-start | bytes 131072 | tf_op jit(solution)/shard_map/all_to_all | solution.py:110
where the time goes:
time: 73.9 us; the launch traced here: 73.3 us
  starting transfers between devices  16.7 us (23%)
  waiting for transfers between devices  16.2 us (22%)
  blocking collectives  15.5 us (21%)
  matrix products  14.9 us (20%)
  local copies, waits for them, and re-layouts  6.73 us (9%)
  other arithmetic  2.94 us (4%)
    all_to_all x1, blocking collectives, body(): lax.all_to_all(spectrum, 'col', split_axis=0, concat_axis=1, tiled=True)  8.3 us
    all_to_all x1, blocking collectives, body(): lax.all_to_all(local_order(returned, row_count), 'row', split_axis=0, con...  7.21 us
    all_to_all x1, waiting for transfers between devices, body(): lax.all_to_all(as_sent(merged_real), 'col', split_axis=1, concat_axis=0,...  5.44 us
    all_to_all x1, starting transfers between devices, body(): lax.all_to_all(as_sent(real_part[None]), 'row', split_axis=2, concat_axis...  5.23 us
    dot_general x1, matrix products, one_block(): jnp.dot(jnp.sin(angles), imag_part, precision=lax.Precision.HIGHEST, pref...  5.11 us
    all_to_all x1, waiting for transfers between devices, body(): lax.all_to_all(as_sent(merged_imag), 'col', split_axis=1, concat_axis=0,...  4.98 us
    all_to_all x1, starting transfers between devices, body(): lax.all_to_all(as_sent(merged_imag), 'col', split_axis=1, concat_axis=0,...  4.88 us
    dot_general x1, matrix products, one_block(): jnp.dot(jnp.cos(angles), real_part, precision=lax.Precision.HIGHEST, pref...  4.73 us
  transfers between devices with their start and end apart: 4, of which 4 were waited for; matrix products, arithmetic and copies ran while one was open for 7% of the time, Pallas kernels for 0%

commit v1 on v0

v1 whole, which is shorter than its diff:
```python
import functools
import math

import jax
import jax.numpy as jnp
import numpy as np
from jax import lax
from jax.experimental import pallas as pl
from jax.experimental.pallas import tpu as pltpu
from jax.sharding import PartitionSpec as P

GROUPS = 4
LANES = 128
MESH = pl.DeviceIdType.MESH


def tables(length, set_count, block, seq_count, chan):
    set_freqs = length // set_count
    half = block // 2
    per_tile = LANES // half
    kappa = np.arange(set_freqs)[:, None]
    lane = np.arange(LANES)[None, :]
    offset = block * (lane // half) + lane % half
    turn = 2.0 * np.pi / length
    angle = turn * (kappa * offset % length)
    base = np.stack([np.cos(angle), np.sin(angle)])
    which = np.arange(set_count)[:, None]
    angle = turn * (which * set_freqs * offset % length)
    phase = np.stack([np.cos(angle), np.sin(angle)], axis=1)
    phase = np.repeat(phase[:, :, None, :], 8, axis=2)
    period = length // (block * per_tile)
    angle = turn * (np.arange(period)[:, None] * block * per_tile % length)
    step = np.stack([np.cos(angle), np.sin(angle)])
    step = np.repeat(step, LANES, axis=2)
    rows = min(set_freqs, length // half)
    scale = 1.0 / math.sqrt(length * chan)
    angle = turn * (np.arange(rows)[:, None] * half % length)
    first = lane < chan
    merge = np.stack(
        [np.where(first, 1.0, np.cos(angle)) * scale, np.where(first, 0.0, np.sin(angle)) * scale]
    )
    index = np.arange(chan)
    angle = 2.0 * np.pi / chan * (index[:, None] * index[None, :] % chan)
    cos, sin, zero = np.cos(angle), np.sin(angle), np.zeros((chan, chan))
    mixer = np.block(
        [
            [cos, zero, zero, zero],
            [zero, cos, zero, -sin],
            [-sin, zero, zero, zero],
            [zero, -sin, zero, -cos],
        ]
    )
    f32 = [jnp.asarray(a, jnp.float32) for a in (base, phase, step, merge)]
    return f32 + [jnp.asarray(mixer, jnp.float32).astype(jnp.bfloat16)]


def kernel(
    row_count, col_count,
    tok_hbm, proj_hbm, gate_hbm, outw_hbm, base_hbm, phase_hbm, step_hbm, merge_hbm, mixer_hbm,
    out_ref,
    tok, proj, gate, outw, base, phase, step, merge, mixer,
    sendbuf, recv, tab, acc, pack, recv2,
    in_sem, send_sem, recv_sem, send2_sem, recv2_sem, own_sem,
):
    seq_count, block, width = tok.shape
    members = sendbuf.shape[0]
    half = block // 2
    chan = LANES // 2
    count = row_count * col_count
    row, col = lax.axis_index("row"), lax.axis_index("col")
    place = row * col_count + col
    order = col * row_count + row
    group_id, member = order // members, order % members

    def device(at):
        at = lax.rem(at, count)
        return (lax.rem(at, row_count), at // row_count)

    barrier = pltpu.get_barrier_semaphore()

    @pl.loop(1, count)
    def _(i):
        pl.semaphore_signal(barrier, inc=1, device_id=device(order + i), device_id_type=MESH)

    loads = [
        pltpu.make_async_copy(src, dst, in_sem.at[i])
        for i, (src, dst) in enumerate(
            [
                (tok_hbm, tok), (proj_hbm, proj), (gate_hbm, gate), (base_hbm, base),
                (phase_hbm.at[group_id], phase), (step_hbm, step), (merge_hbm, merge),
                (mixer_hbm, mixer), (outw_hbm, outw),
            ]
        )
    ]
    for load in loads:
        load.start()
    for load in loads[:3]:
        load.wait()

    flat = tok[...].reshape(seq_count * block, width)
    hidden = jnp.dot(flat, proj[...], preferred_element_type=jnp.float32)
    hidden = hidden.astype(jnp.bfloat16).astype(jnp.float32)
    gate_pre = jnp.dot(flat, gate[...], preferred_element_type=jnp.float32)
    mix = hidden * (gate_pre / (1.0 + jnp.exp(-gate_pre)))
    low = lax.broadcasted_iota(jnp.int32, (half, LANES), 1) < chan
    for s in range(seq_count):
        for t in range(GROUPS // 2):
            top = mix[s * block : s * block + half, t * LANES : (t + 1) * LANES]
            bottom = mix[s * block + half : (s + 1) * block, t * LANES : (t + 1) * LANES]
            even = jnp.where(low, top, pltpu.roll(bottom, chan, 1))
            odd = jnp.where(low, pltpu.roll(top, chan, 1), bottom)
            sendbuf[s * GROUPS + 2 * t] = even.astype(jnp.bfloat16)
            sendbuf[s * GROUPS + 2 * t + 1] = odd.astype(jnp.bfloat16)

    pl.semaphore_wait(barrier, count - 1)

    def copy_to(at):
        at = lax.rem(at, count)
        return pltpu.make_async_remote_copy(
            src_ref=sendbuf.at[lax.rem(at, members)],
            dst_ref=recv.at[place],
            send_sem=send_sem.at[at],
            recv_sem=recv_sem.at[place],
            device_id=device(at),
            device_id_type=MESH,
        )

    own = pltpu.make_async_copy(sendbuf.at[member], recv.at[place], own_sem)

    @pl.loop(1, count)
    def _(i):
        copy_to(order + lax.rem(i + count // 2 - 1, count - 1) + 1).start()

    own.start()

    for load in loads[3:]:
        load.wait()
    base_cos, base_sin = base[0], base[1]
    set_freqs = base_cos.shape[0]
    lane_cos, lane_sin = phase[0][:1], phase[1][:1]
    turned_cos = base_cos * lane_cos - base_sin * lane_sin
    turned_sin = base_sin * lane_cos + base_cos * lane_sin
    base[0], base[1] = turned_cos, turned_sin
    chunks, _, depth = tab.shape
    per_chunk = depth // LANES
    period = step.shape[1]
    step_cos, step_sin = step[0], step[1]

    def fill(c, now):
        for t in range(per_chunk):
            now_cos, now_sin = now
            bc = base[0].reshape(set_freqs // period, period, LANES)
            bs = base[1].reshape(set_freqs // period, period, LANES)
            tc = (bc * now_cos[None] - bs * now_sin[None]).reshape(set_freqs, LANES)
            ts = (bs * now_cos[None] + bc * now_sin[None]).reshape(set_freqs, LANES)
            tab[c, :set_freqs, t * LANES : (t + 1) * LANES] = tc.astype(jnp.bfloat16)
            tab[c, set_freqs:, t * LANES : (t + 1) * LANES] = ts.astype(jnp.bfloat16)
            now = (
                now_cos * step_cos - now_sin * step_sin,
                now_sin * step_cos + now_cos * step_sin,
            )
        return now

    start = (jnp.ones_like(step_cos), jnp.zeros_like(step_sin))
    lax.fori_loop(0, chunks, fill, start)

    own.wait()

    @pl.loop(1, count)
    def _(i):
        source = lax.rem(place + i, count)
        pltpu.make_async_remote_copy(
            src_ref=sendbuf.at[0],
            dst_ref=recv.at[source],
            send_sem=send_sem.at[0],
            recv_sem=recv_sem.at[source],
            device_id=(row, col),
            device_id_type=MESH,
        ).wait_recv()

    sources = depth // half

    def part(c):
        data = recv[pl.ds(c * sources, sources)].reshape(depth, LANES)
        return jnp.dot(tab[c], data, preferred_element_type=jnp.float32)

    if chunks == 1:
        total = part(0)
    else:
        acc[...] = part(0)

        @pl.loop(1, chunks)
        def _(c):
            acc[...] += part(c)

        total = acc[...]
    both = jnp.concatenate([total[:set_freqs], total[set_freqs:]], axis=1).astype(jnp.bfloat16)
    mixed = jnp.dot(both, mixer[...], preferred_element_type=jnp.float32)
    rows = merge.shape[1]
    kept = mixed[:, :LANES].reshape(set_freqs // rows, rows, LANES) * merge[0][None]
    kept = kept + mixed[:, LANES:].reshape(set_freqs // rows, rows, LANES) * merge[1][None]
    kept = kept.reshape(set_freqs, LANES)
    kept = kept + pltpu.roll(kept, chan, 1)
    for b in range(members):
        top = kept[b * block : b * block + half]
        bottom = kept[b * block + half : (b + 1) * block]
        pack[b] = jnp.where(low, top, bottom).astype(jnp.bfloat16)

    def back_to(b):
        return pltpu.make_async_remote_copy(
            src_ref=pack.at[b],
            dst_ref=recv2.at[member],
            send_sem=send2_sem.at[b],
            recv_sem=recv2_sem.at[member],
            device_id=device(group_id * members + b),
            device_id_type=MESH,
        )

    @pl.loop(1, members)
    def _(i):
        back_to(lax.rem(member + i, members)).start()

    own2 = pltpu.make_async_copy(pack.at[member], recv2.at[member], own_sem)
    own2.start()

    @pl.loop(1, count)
    def _(i):
        copy_to(order + i).wait_send()

    own2.wait()

    @pl.loop(1, members)
    def _(i):
        source = lax.rem(member + i, members)
        pltpu.make_async_remote_copy(
            src_ref=pack.at[0],
            dst_ref=recv2.at[source],
            send_sem=send2_sem.at[0],
            recv_sem=recv2_sem.at[source],
            device_id=(row, col),
            device_id_type=MESH,
        ).wait_recv()

    for s in range(seq_count):
        tops, bottoms = [], []
        for t in range(GROUPS // 2):
            even = recv2[s * GROUPS + 2 * t].astype(jnp.float32)
            odd = recv2[s * GROUPS + 2 * t + 1].astype(jnp.float32)
            tops.append(jnp.where(low, even, pltpu.roll(odd, chan, 1)))
            bottoms.append(jnp.where(low, pltpu.roll(even, chan, 1), odd))
        lhs = jnp.concatenate(
            [jnp.concatenate(tops, axis=1), jnp.concatenate(bottoms, axis=1)], axis=0
        ).astype(jnp.bfloat16)
        out_ref[s] = jnp.dot(lhs, outw[...], preferred_element_type=jnp.float32).astype(
            jnp.bfloat16
        )

    @pl.loop(1, members)
    def _(i):
        back_to(lax.rem(member + i, members)).wait_send()


def body(row_count, col_count, tokens, proj_weight, gate_weight, out_weight):
    seq_count, block, width = tokens.shape
    mixer_width = proj_weight.shape[1]
    chan = mixer_width // GROUPS
    members = seq_count * GROUPS
    count = row_count * col_count
    length = count * block
    set_count = count // members
    set_freqs = members * block
    half = block // 2
    consts = tables(length, set_count, block, seq_count, chan)
    base, phase, step, merge, mixer = consts
    depth = min(1024, count * half)
    chunks = count * half // depth
    bf16, f32 = jnp.bfloat16, jnp.float32
    dma = pltpu.SemaphoreType.DMA
    return pl.pallas_call(
        functools.partial(kernel, row_count, col_count),
        out_shape=jax.ShapeDtypeStruct((seq_count, block, out_weight.shape[1]), bf16),
        in_specs=[pl.BlockSpec(memory_space=pl.ANY)] * 9,
        out_specs=pl.BlockSpec(memory_space=pltpu.VMEM),
        scratch_shapes=[
            pltpu.VMEM(tokens.shape, bf16),
            pltpu.VMEM(proj_weight.shape, bf16),
            pltpu.VMEM(gate_weight.shape, bf16),
            pltpu.VMEM(out_weight.shape, bf16),
            pltpu.VMEM(base.shape, f32),
            pltpu.VMEM(phase.shape[1:], f32),
            pltpu.VMEM(step.shape, f32),
            pltpu.VMEM(merge.shape, f32),
            pltpu.VMEM(mixer.shape, bf16),
            pltpu.VMEM((members, half, LANES), bf16),
            pltpu.VMEM((count, half, LANES), bf16),
            pltpu.VMEM((chunks, 2 * set_freqs, depth), bf16),
            pltpu.VMEM((2 * set_freqs, LANES), f32),
            pltpu.VMEM((members, half, LANES), bf16),
            pltpu.VMEM((members, half, LANES), bf16),
            dma((9,)),
            dma((count,)),
            dma((count,)),
            dma((members,)),
            dma((members,)),
            dma,
        ],
        compiler_params=pltpu.CompilerParams(
            collective_id=0, has_side_effects=True, vmem_limit_bytes=56 * 1024 * 1024
        ),
    )(tokens, proj_weight, gate_weight, out_weight, *consts)


def solution(mesh):
    in_specs = (P(None, ("row", "col"), None), P(), P(), P())
    out_specs = P(None, ("col", "row"), None)
    run = functools.partial(body, mesh.shape["row"], mesh.shape["col"])
    return jax.shard_map(run, mesh=mesh, in_specs=in_specs, out_specs=out_specs, check_vma=False)
```

time: 73.9 us -> 22.8 us (0.31)
  Pallas kernels: 0 us -> 21 us
  starting transfers between devices: 16.7 us -> 0 us
  waiting for transfers between devices: 16.2 us -> 0 us
  blocking collectives: 15.5 us -> 0 us
  matrix products: 14.9 us -> 0 us
  local copies, waits for them, and re-layouts: 6.73 us -> 1.67 us
  other arithmetic: 2.94 us -> 0 us
    pallas_call x0 -> x1, Pallas kernels: none -> 21 us  [body(): pl.pallas_call(functools.partial(kernel, row_count, col_count), out_shape...]
    all_to_all x4 -> x0, starting transfers between devices: 16.7 us -> none  [the longest x1 5.23 us: body(): lax.all_to_all(as_sent(real_part[None]), 'row', split_axis=2, concat_axis...]
    all_to_all x4 -> x0, waiting for transfers between devices: 16.2 us -> none  [the longest x1 5.44 us: body(): lax.all_to_all(as_sent(merged_real), 'col', split_axis=1, concat_axis=0,...]
    all_to_all x2 -> x0, blocking collectives: 15.5 us -> none  [the longest x1 8.3 us: body(): lax.all_to_all(spectrum, 'col', split_axis=0, concat_axis=1, tiled=True)]
    dot_general x11 -> x0, matrix products: 14.9 us -> none  [the longest x1 5.11 us: one_block(): jnp.dot(jnp.sin(angles), imag_part, precision=lax.Precision.HIGHEST, pref...]
    unnamed x17 -> x1, local copies, waits for them, and re-layouts: 4.56 us -> 1.67 us
    unnamed x2 -> x0, other arithmetic: 2.89 us -> none
    all_to_all x13 -> x0, local copies, waits for them, and re-layouts: 1.01 us -> none  [the longest x3 0.25 us: body(): lax.all_to_all(as_sent(merged_imag), 'col', split_axis=1, concat_axis=0,...]
  transfers between devices with their start and end apart: 4 -> 0, of which waited for: 4 -> 0; matrix products, arithmetic and copies ran while one was open for 7% -> 0% of each run, Pallas kernels for 0% -> 0%
where the time goes in v1:
time: 22.8 us; the launch traced here: 22.7 us
  Pallas kernels  21 us (92%)
  local copies, waits for them, and re-layouts  1.67 us (7%)
    pallas_call x1, Pallas kernels, body(): pl.pallas_call(functools.partial(kernel, row_count, col_count), out_shape...  21 us
    unnamed x1, local copies, waits for them, and re-layouts  1.67 us

profile of v1, /device:TPU:0, one launch (start us, length us, event | category | flops | bytes accessed | tf_op | source)
XLA Modules:
  0.0 22.7 jit_solution(5015997479289839763)
XLA Ops:
  0.0 21.0 %shard_map.91 = bf16[2,64,1024]{2,1,0:T(8,128)(2,1)} custom-call(bf16[2,64,1024]{2,1,0:T(8,128)(2,1)} %tok_hbm.1, bf16[1024,256]{1,0:T(8,128)(2,1)} %proj_hbm.1, bf16[1024,256]{1,0:T(8,128)(2,1)} %gate_hbm.1, bf16[256,1024]{1,0:T(8,128)(2,1)} %outw_hbm.1, f32[2,512,128]{2,1,0:T(8,128)} %constant.10.clone.base_hbm, ...), custom_call_target="tpu_custom_call" | custom-call | tf_op jit(solution)/shard_map/pallas_call | solution.py:279
  21.0 1.7 %copy.11 = bf16[2,64,1024]{2,1,0:T(8,128)(2,1)} copy(bf16[2,64,1024]{2,1,0:T(8,128)(2,1)} %shard_map.91) | data formatting | bytes 524288

commit v2 on v1

--- a/solution.py
+++ b/solution.py
@@ -56,9 +56,9 @@
 
 def kernel(
     row_count, col_count,
-    tok_hbm, proj_hbm, gate_hbm, outw_hbm, base_hbm, phase_hbm, step_hbm, merge_hbm, mixer_hbm,
+    tok_hbm, proj_hbm, gate_hbm, base_hbm, phase_hbm, step_hbm, merge_hbm, mixer_hbm,
     out_ref,
-    tok, proj, gate, outw, base, phase, step, merge, mixer,
+    tok, proj, gate, base, phase, step, merge, mixer,
     sendbuf, recv, tab, acc, pack, recv2,
     in_sem, send_sem, recv_sem, send2_sem, recv2_sem, own_sem,
 ):
@@ -88,7 +88,7 @@
             [
                 (tok_hbm, tok), (proj_hbm, proj), (gate_hbm, gate), (base_hbm, base),
                 (phase_hbm.at[group_id], phase), (step_hbm, step), (merge_hbm, merge),
-                (mixer_hbm, mixer), (outw_hbm, outw),
+                (mixer_hbm, mixer),
             ]
         )
     ]
@@ -129,7 +129,7 @@
 
     @pl.loop(1, count)
     def _(i):
-        copy_to(order + lax.rem(i + count // 2 - 1, count - 1) + 1).start()
+        copy_to(order + i).start()
 
     own.start()
 
@@ -164,6 +164,7 @@
     start = (jnp.ones_like(step_cos), jnp.zeros_like(step_sin))
     lax.fori_loop(0, chunks, fill, start)
 
+
     own.wait()
 
     @pl.loop(1, count)
@@ -251,9 +252,7 @@
         lhs = jnp.concatenate(
             [jnp.concatenate(tops, axis=1), jnp.concatenate(bottoms, axis=1)], axis=0
         ).astype(jnp.bfloat16)
-        out_ref[s] = jnp.dot(lhs, outw[...], preferred_element_type=jnp.float32).astype(
-            jnp.bfloat16
-        )
+        out_ref[s] = lhs
 
     @pl.loop(1, members)
     def _(i):
@@ -276,16 +275,15 @@
     chunks = count * half // depth
     bf16, f32 = jnp.bfloat16, jnp.float32
     dma = pltpu.SemaphoreType.DMA
-    return pl.pallas_call(
+    mixed = pl.pallas_call(
         functools.partial(kernel, row_count, col_count),
-        out_shape=jax.ShapeDtypeStruct((seq_count, block, out_weight.shape[1]), bf16),
-        in_specs=[pl.BlockSpec(memory_space=pl.ANY)] * 9,
+        out_shape=jax.ShapeDtypeStruct((seq_count, block, mixer_width), bf16),
+        in_specs=[pl.BlockSpec(memory_space=pl.ANY)] * 8,
         out_specs=pl.BlockSpec(memory_space=pltpu.VMEM),
         scratch_shapes=[
             pltpu.VMEM(tokens.shape, bf16),
             pltpu.VMEM(proj_weight.shape, bf16),
             pltpu.VMEM(gate_weight.shape, bf16),
-            pltpu.VMEM(out_weight.shape, bf16),
             pltpu.VMEM(base.shape, f32),
             pltpu.VMEM(phase.shape[1:], f32),
             pltpu.VMEM(step.shape, f32),
@@ -297,7 +295,7 @@
             pltpu.VMEM((2 * set_freqs, LANES), f32),
             pltpu.VMEM((members, half, LANES), bf16),
             pltpu.VMEM((members, half, LANES), bf16),
-            dma((9,)),
+            dma((8,)),
             dma((count,)),
             dma((count,)),
             dma((members,)),
@@ -305,9 +303,11 @@
             dma,
         ],
         compiler_params=pltpu.CompilerParams(
-            collective_id=0, has_side_effects=True, vmem_limit_bytes=56 * 1024 * 1024
+            collective_id=0, has_side_effects=True, vmem_limit_bytes=60 * 1024 * 1024
         ),
-    )(tokens, proj_weight, gate_weight, out_weight, *consts)
+    )(tokens, proj_weight, gate_weight, *consts)
+    result = jnp.einsum("stc,cd->std", mixed, out_weight, preferred_element_type=jnp.float32)
+    return result.astype(bf16)
 
 
 def solution(mesh):

time: 22.8 us -> 20.8 us (0.912)
  Pallas kernels: 21 us -> 18.8 us
  matrix products: 0 us -> 1.78 us
  local copies, waits for them, and re-layouts: 1.67 us -> 0.01 us
    pallas_call x1, Pallas kernels: 21 us -> 18.8 us  [body(): pl.pallas_call(functools.partial(kernel, row_count, col_count), out_shape...]
    dot_general x0 -> x1, matrix products: none -> 1.78 us  [body(): jnp.einsum('stc,cd->std', mixed, out_weight, preferred_element_type=jnp.f...]
    unnamed x1 -> x2, local copies, waits for them, and re-layouts: 1.67 us -> 0.01 us
where the time goes in v2:
time: 20.8 us; the launch traced here: 20.7 us
  Pallas kernels  18.8 us (90%)
  matrix products  1.78 us (9%)
    pallas_call x1, Pallas kernels, body(): pl.pallas_call(functools.partial(kernel, row_count, col_count), out_shape...  18.8 us
    dot_general x1, matrix products, body(): jnp.einsum('stc,cd->std', mixed, out_weight, preferred_element_type=jnp.f...  1.78 us

profile of v2, /device:TPU:0, one launch (start us, length us, event | category | flops | bytes accessed | tf_op | source)
XLA Modules:
  0.0 20.7 jit_solution(12166359613958601942)
XLA Ops:
  0.0 0.0 copy-start
  0.0 18.8 %shard_map.91 = bf16[2,64,256]{2,1,0:T(8,128)(2,1)} custom-call(bf16[2,64,1024]{2,1,0:T(8,128)(2,1)} %tok_hbm.1, bf16[1024,256]{1,0:T(8,128)(2,1)} %proj_hbm.1, bf16[1024,256]{1,0:T(8,128)(2,1)} %gate_hbm.1, f32[2,512,128]{2,1,0:T(8,128)} %constant.10.clone.base_hbm, f32[4,2,8,128]{3,2,1,0:T(8,128)} %constant.11.clone.phase_hbm, ...), custom_call_target="tpu_custom_call" | custom-call | tf_op jit(solution)/shard_map/pallas_call | solution.py:278
  18.9 0.0 copy-done
  18.9 1.8 %convolution_convert_fusion = bf16[2,64,1024]{2,1,0:T(8,128)(2,1)} fusion(bf16[2,64,256]{2,1,0:T(8,128)(2,1)} %shard_map.91, bf16[256,1024]{1,0:T(8,128)(2,1)S(1)} %copy-done), kind=kOutput, calls=%fused_computation | convolution fusion | flops 67239936 | bytes 851968 | tf_op jit(solution)/shard_map/stc,cd->std/dot_general | solution.py:309
Async XLA Ops:
  0.0 18.9 %copy-start = (bf16[256,1024]{1,0:T(8,128)(2,1)S(1)}, bf16[256,1024]{1,0:T(8,128)(2,1)}, u32[]{:S(2)}) copy-start(bf16[256,1024]{1,0:T(8,128)(2,1)} %param.12) | copy-start | bytes 1572868

commit v3 on v2

--- a/solution.py
+++ b/solution.py
@@ -50,15 +50,16 @@
             [zero, -sin, zero, -cos],
         ]
     )
-    f32 = [jnp.asarray(a, jnp.float32) for a in (base, phase, step, merge)]
-    return f32 + [jnp.asarray(mixer, jnp.float32).astype(jnp.bfloat16)]
+    mixer = np.concatenate([mixer[:, :LANES], mixer[:, LANES:]])
+    parts = [a.reshape(-1, LANES) for a in (base, step, merge, mixer, phase)]
+    return jnp.asarray(np.concatenate(parts), jnp.float32), period, rows
 
 
 def kernel(
-    row_count, col_count,
-    tok_hbm, proj_hbm, gate_hbm, base_hbm, phase_hbm, step_hbm, merge_hbm, mixer_hbm,
+    row_count, col_count, period, rows,
+    tok_hbm, proj_hbm, gate_hbm, table_hbm,
     out_ref,
-    tok, proj, gate, base, phase, step, merge, mixer,
+    tok, proj, gate, table,
     sendbuf, recv, tab, acc, pack, recv2,
     in_sem, send_sem, recv_sem, send2_sem, recv2_sem, own_sem,
 ):
@@ -86,9 +87,7 @@
         pltpu.make_async_copy(src, dst, in_sem.at[i])
         for i, (src, dst) in enumerate(
             [
-                (tok_hbm, tok), (proj_hbm, proj), (gate_hbm, gate), (base_hbm, base),
-                (phase_hbm.at[group_id], phase), (step_hbm, step), (merge_hbm, merge),
-                (mixer_hbm, mixer),
+                (tok_hbm, tok), (proj_hbm, proj), (gate_hbm, gate), (table_hbm, table),
             ]
         )
     ]
@@ -129,28 +128,34 @@
 
     @pl.loop(1, count)
     def _(i):
-        copy_to(order + i).start()
+        copy_to(order + lax.rem(i + 2, count - 1) + 1).start()
 
     own.start()
 
     for load in loads[3:]:
         load.wait()
-    base_cos, base_sin = base[0], base[1]
-    set_freqs = base_cos.shape[0]
-    lane_cos, lane_sin = phase[0][:1], phase[1][:1]
+    chunks, set_freqs, depth = tab.shape
+    set_freqs = set_freqs // 2
+    base_cos, base_sin = table[:set_freqs], table[set_freqs : 2 * set_freqs]
+    step_at = 2 * set_freqs
+    merge_at = step_at + 2 * period
+    mixer_at = merge_at + 2 * rows
+    phase_at = mixer_at + 4 * LANES
+    lane_cos = table[pl.ds(phase_at + group_id * 16, 8)][:1]
+    lane_sin = table[pl.ds(phase_at + group_id * 16 + 8, 8)][:1]
     turned_cos = base_cos * lane_cos - base_sin * lane_sin
     turned_sin = base_sin * lane_cos + base_cos * lane_sin
-    base[0], base[1] = turned_cos, turned_sin
-    chunks, _, depth = tab.shape
+    table[:set_freqs] = turned_cos
+    table[set_freqs : 2 * set_freqs] = turned_sin
     per_chunk = depth // LANES
-    period = step.shape[1]
-    step_cos, step_sin = step[0], step[1]
+    step_cos = table[step_at : step_at + period]
+    step_sin = table[step_at + period : merge_at]
 
     def fill(c, now):
         for t in range(per_chunk):
             now_cos, now_sin = now
-            bc = base[0].reshape(set_freqs // period, period, LANES)
-            bs = base[1].reshape(set_freqs // period, period, LANES)
+            bc = table[:set_freqs].reshape(set_freqs // period, period, LANES)
+            bs = table[set_freqs : 2 * set_freqs].reshape(set_freqs // period, period, LANES)
             tc = (bc * now_cos[None] - bs * now_sin[None]).reshape(set_freqs, LANES)
             ts = (bs * now_cos[None] + bc * now_sin[None]).reshape(set_freqs, LANES)
             tab[c, :set_freqs, t * LANES : (t + 1) * LANES] = tc.astype(jnp.bfloat16)
@@ -196,10 +201,12 @@
 
         total = acc[...]
     both = jnp.concatenate([total[:set_freqs], total[set_freqs:]], axis=1).astype(jnp.bfloat16)
-    mixed = jnp.dot(both, mixer[...], preferred_element_type=jnp.float32)
-    rows = merge.shape[1]
-    kept = mixed[:, :LANES].reshape(set_freqs // rows, rows, LANES) * merge[0][None]
-    kept = kept + mixed[:, LANES:].reshape(set_freqs // rows, rows, LANES) * merge[1][None]
+    mixer = [table[mixer_at + 2 * LANES * i : mixer_at + 2 * LANES * (i + 1)] for i in (0, 1)]
+    mixer = jnp.concatenate(mixer, axis=1).astype(jnp.bfloat16)
+    mixed = jnp.dot(both, mixer, preferred_element_type=jnp.float32)
+    keep, turn = table[merge_at : merge_at + rows], table[merge_at + rows : mixer_at]
+    kept = mixed[:, :LANES].reshape(set_freqs // rows, rows, LANES) * keep[None]
+    kept = kept + mixed[:, LANES:].reshape(set_freqs // rows, rows, LANES) * turn[None]
     kept = kept.reshape(set_freqs, LANES)
     kept = kept + pltpu.roll(kept, chan, 1)
     for b in range(members):
@@ -269,33 +276,28 @@
     set_count = count // members
     set_freqs = members * block
     half = block // 2
-    consts = tables(length, set_count, block, seq_count, chan)
-    base, phase, step, merge, mixer = consts
+    table, period, rows = tables(length, set_count, block, seq_count, chan)
     depth = min(1024, count * half)
     chunks = count * half // depth
     bf16, f32 = jnp.bfloat16, jnp.float32
     dma = pltpu.SemaphoreType.DMA
     mixed = pl.pallas_call(
-        functools.partial(kernel, row_count, col_count),
+        functools.partial(kernel, row_count, col_count, period, rows),
         out_shape=jax.ShapeDtypeStruct((seq_count, block, mixer_width), bf16),
-        in_specs=[pl.BlockSpec(memory_space=pl.ANY)] * 8,
+        in_specs=[pl.BlockSpec(memory_space=pl.ANY)] * 4,
         out_specs=pl.BlockSpec(memory_space=pltpu.VMEM),
         scratch_shapes=[
             pltpu.VMEM(tokens.shape, bf16),
             pltpu.VMEM(proj_weight.shape, bf16),
             pltpu.VMEM(gate_weight.shape, bf16),
-            pltpu.VMEM(base.shape, f32),
-            pltpu.VMEM(phase.shape[1:], f32),
-            pltpu.VMEM(step.shape, f32),
-            pltpu.VMEM(merge.shape, f32),
-            pltpu.VMEM(mixer.shape, bf16),
+            pltpu.VMEM(table.shape, f32),
             pltpu.VMEM((members, half, LANES), bf16),
             pltpu.VMEM((count, half, LANES), bf16),
             pltpu.VMEM((chunks, 2 * set_freqs, depth), bf16),
             pltpu.VMEM((2 * set_freqs, LANES), f32),
             pltpu.VMEM((members, half, LANES), bf16),
             pltpu.VMEM((members, half, LANES), bf16),
-            dma((8,)),
+            dma((4,)),
             dma((count,)),
             dma((count,)),
             dma((members,)),
@@ -303,9 +305,9 @@
             dma,
         ],
         compiler_params=pltpu.CompilerParams(
-            collective_id=0, has_side_effects=True, vmem_limit_bytes=60 * 1024 * 1024
+            collective_id=0, has_side_effects=True, vmem_limit_bytes=56360960
         ),
-    )(tokens, proj_weight, gate_weight, *consts)
+    )(tokens, proj_weight, gate_weight, table)
     result = jnp.einsum("stc,cd->std", mixed, out_weight, preferred_element_type=jnp.float32)
     return result.astype(bf16)
 

time: 20.8 us -> 19.3 us (0.928)
  matrix products: 1.78 us -> 0.94 us
  Pallas kernels: 18.8 us -> 18.2 us
    dot_general x1, matrix products: 1.78 us -> 0.94 us  [body(): jnp.einsum('stc,cd->std', mixed, out_weight, preferred_element_type=jnp.f...]
    pallas_call x1, Pallas kernels: 18.8 us -> 18.2 us  [body(): pl.pallas_call(functools.partial(kernel, row_count, col_count, period, ro...]
where the time goes in v3:
time: 19.3 us; the launch traced here: 19.1 us
  Pallas kernels  18.2 us (94%)
  matrix products  0.94 us (5%)
    pallas_call x1, Pallas kernels, body(): pl.pallas_call(functools.partial(kernel, row_count, col_count, period, ro...  18.2 us
    dot_general x1, matrix products, body(): jnp.einsum('stc,cd->std', mixed, out_weight, preferred_element_type=jnp.f...  0.94 us

profile of v3, /device:TPU:0, one launch (start us, length us, event | category | flops | bytes accessed | tf_op | source)
XLA Modules:
  0.0 19.1 jit_solution(14320030764418550082)
XLA Ops:
  0.0 0.0 copy-start
  0.0 18.2 %shard_map.55 = bf16[2,64,256]{2,1,0:T(8,128)(2,1)S(1)} custom-call(bf16[2,64,1024]{2,1,0:T(8,128)(2,1)} %tok_hbm.1, bf16[1024,256]{1,0:T(8,128)(2,1)} %proj_hbm.1, bf16[1024,256]{1,0:T(8,128)(2,1)} %gate_hbm.1, f32[1744,128]{1,0:T(8,128)} %constant.2.clone.table_hbm), custom_call_target="tpu_custom_call" | custom-call | tf_op jit(solution)/shard_map/pallas_call | solution.py:284
  18.2 0.0 copy-done
  18.2 0.9 %convolution_convert_fusion = bf16[2,64,1024]{2,1,0:T(8,128)(2,1)} fusion(bf16[2,64,256]{2,1,0:T(8,128)(2,1)S(1)} %shard_map.55, bf16[256,1024]{1,0:T(8,128)(2,1)S(1)} %copy-done), kind=kOutput, calls=%fused_computation | convolution fusion | flops 67239936 | bytes 851968 | tf_op jit(solution)/shard_map/stc,cd->std/dot_general | solution.py:311
Async XLA Ops:
  0.0 18.2 %copy-start = (bf16[256,1024]{1,0:T(8,128)(2,1)S(1)}, bf16[256,1024]{1,0:T(8,128)(2,1)}, u32[]{:S(2)}) copy-start(bf16[256,1024]{1,0:T(8,128)(2,1)} %param.8) | copy-start | bytes 1572868

commit v4 on v3

--- a/solution.py
+++ b/solution.py
@@ -209,11 +209,6 @@
     kept = kept + mixed[:, LANES:].reshape(set_freqs // rows, rows, LANES) * turn[None]
     kept = kept.reshape(set_freqs, LANES)
     kept = kept + pltpu.roll(kept, chan, 1)
-    for b in range(members):
-        top = kept[b * block : b * block + half]
-        bottom = kept[b * block + half : (b + 1) * block]
-        pack[b] = jnp.where(low, top, bottom).astype(jnp.bfloat16)
-
     def back_to(b):
         return pltpu.make_async_remote_copy(
             src_ref=pack.at[b],
@@ -224,9 +219,14 @@
             device_id_type=MESH,
         )
 
-    @pl.loop(1, members)
-    def _(i):
-        back_to(lax.rem(member + i, members)).start()
+    for b in range(members):
+        top = kept[b * block : b * block + half]
+        bottom = kept[b * block + half : (b + 1) * block]
+        pack[b] = jnp.where(low, top, bottom).astype(jnp.bfloat16)
+
+        @pl.when(b != member)
+        def _():
+            back_to(b).start()
 
     own2 = pltpu.make_async_copy(pack.at[member], recv2.at[member], own_sem)
     own2.start()

time: 19.3 us -> 19.1 us (0.990)
  Pallas kernels: 18.2 us -> 18 us
where the time goes in v4:
time: 19.1 us; the launch traced here: 19 us
  Pallas kernels  18 us (94%)
  matrix products  0.94 us (5%)
    pallas_call x1, Pallas kernels, body(): pl.pallas_call(functools.partial(kernel, row_count, col_count, period, ro...  18 us
    dot_general x1, matrix products, body(): jnp.einsum('stc,cd->std', mixed, out_weight, preferred_element_type=jnp.f...  0.94 us

profile of v4, /device:TPU:0, one launch (start us, length us, event | category | flops | bytes accessed | tf_op | source)
XLA Modules:
  0.0 19.0 jit_solution(10754834723121999378)
XLA Ops:
  0.0 0.0 copy-start
  0.0 18.0 %shard_map.55 = bf16[2,64,256]{2,1,0:T(8,128)(2,1)S(1)} custom-call(bf16[2,64,1024]{2,1,0:T(8,128)(2,1)} %tok_hbm.1, bf16[1024,256]{1,0:T(8,128)(2,1)} %proj_hbm.1, bf16[1024,256]{1,0:T(8,128)(2,1)} %gate_hbm.1, f32[1744,128]{1,0:T(8,128)} %constant.2.clone.table_hbm), custom_call_target="tpu_custom_call" | custom-call | tf_op jit(solution)/shard_map/pallas_call | solution.py:284
  18.1 0.0 copy-done
  18.1 0.9 %convolution_convert_fusion = bf16[2,64,1024]{2,1,0:T(8,128)(2,1)} fusion(bf16[2,64,256]{2,1,0:T(8,128)(2,1)S(1)} %shard_map.55, bf16[256,1024]{1,0:T(8,128)(2,1)S(1)} %copy-done), kind=kOutput, calls=%fused_computation | convolution fusion | flops 67239936 | bytes 851968 | tf_op jit(solution)/shard_map/stc,cd->std/dot_general | solution.py:311
Async XLA Ops:
  0.0 18.1 %copy-start = (bf16[256,1024]{1,0:T(8,128)(2,1)S(1)}, bf16[256,1024]{1,0:T(8,128)(2,1)}, u32[]{:S(2)}) copy-start(bf16[256,1024]{1,0:T(8,128)(2,1)} %param.8) | copy-start | bytes 1572868
